TPU v7x, 32 devices: a whole 2x2x4 slice. The times are simulated.
32 devices in a mesh: fs: 16 (over z, y, x), tp: 2 (over core).
Axes of the slice: x: 2, y: 2, z: 4, core: 2. Of those that a mesh axis runs over, the one named last changes fastest.
Arguments:
- residual_in: bfloat16 [4096, 2048], P(('fs', 'tp')), may hold values from -6 to 6
- gain_first: float32 [2048], replicated, may hold values from 0.1 to 1.9
- gain_mixer: float32 [2048], replicated, may hold values from 0.1 to 1.9
- gain_second: float32 [2048], replicated, may hold values from 0.1 to 1.9
- gate_weight: float32 [2048, 6144], P('fs', 'tp'), may hold values from -0.125 to 0.125
- gate_scale: float32 [6144], P('tp'), may hold values from 0.3 to 3
- up_weight: float32 [2048, 6144], P('fs', 'tp'), may hold values from -0.125 to 0.125
- up_scale: float32 [6144], P('tp'), may hold values from 0.3 to 3
- down_weight: float32 [6144, 2048], P('tp', 'fs'), may hold values from -0.078125 to 0.078125
- down_scale: float32 [2048], P('fs'), may hold values from 0.3 to 3
- query_weight: float32 [2048, 2048], P('fs', 'tp'), may hold values from -0.125 to 0.125
- query_scale: float32 [2048], P('tp'), may hold values from 0.3 to 3
- key_weight: float32 [2048, 2048], P('fs', 'tp'), may hold values from -0.125 to 0.125
- key_scale: float32 [2048], P('tp'), may hold values from 0.3 to 3
- value_weight: float32 [2048, 2048], P('fs', 'tp'), may hold values from -0.125 to 0.125
- value_scale: float32 [2048], P('tp'), may hold values from 0.3 to 3
- output_weight: float32 [2048, 2048], P('tp', 'fs'), may hold values from -0.125 to 0.125
- output_scale: float32 [2048], P('fs'), may hold values from 0.3 to 3
Outputs:
- residual_out: bfloat16 [4096, 2048], P(('fs', 'tp'))
All inputs are finite; a program needn't handle non-finite values.
Results may differ from a plain program's by a relative error of at most 0.028.
Values may be sent and summed in bfloat16 or wider, within the bound.
A program may use at most 128 MiB of HBM per device.

v0:
```python
import jax
import jax.numpy as jnp
from jax import lax
from jax.sharding import PartitionSpec as P

HEADS = 8
HEAD_DIM = 256
BLOCK = 64


EPSILON = 1e-06
HEAD_FLOOR = 0.25
ROTARY_BASE = 10000.0
HIGHEST = lax.Precision.HIGHEST


def normalize(sequence_rows, gain_vector):
    values = sequence_rows.astype(jnp.float32)
    scaled = values * lax.rsqrt(jnp.mean(values * values, axis=-1, keepdims=True) + EPSILON)
    return (scaled * gain_vector).astype(jnp.bfloat16)


def collect_rows(sequence_rows, gain_vector):
    return lax.all_gather(normalize(sequence_rows, gain_vector), "tp", axis=0, tiled=True)


def return_rows(inputs, weight, factor):
    term = jnp.dot(inputs, weight, preferred_element_type=jnp.float32) * factor
    return lax.psum_scatter(
        lax.optimization_barrier(term.astype(jnp.bfloat16))
        .astype(jnp.float32)
        .astype(jnp.bfloat16),
        "tp",
        scatter_dimension=0,
        tiled=True,
    ).astype(jnp.float32)


def head_rates(first_head, head_count, length):
    head_number = (first_head + jnp.arange(head_count)).astype(jnp.float32)
    return jnp.exp(jnp.log(1.0 / 16.0) + head_number / (HEADS - 1) * jnp.log(4.0 / length))


def rotate(values, positions):
    half_width = values.shape[-1] // 2
    frequency = ROTARY_BASE ** (-jnp.arange(half_width, dtype=jnp.float32) * 2.0 / values.shape[-1])
    angles = positions[:, None] * frequency[None, :]
    cosine = jnp.cos(angles)[:, None, :]
    sine_value = jnp.sin(angles)[:, None, :]
    front_half = values[..., :half_width]
    back_half = values[..., half_width:]
    return jnp.concatenate(
        [
            front_half * cosine - back_half * sine_value,
            back_half * cosine + front_half * sine_value,
        ],
        axis=-1,
    )


def retention(query_pre, key_pre, value_pre, decay_rates):
    length, head_count, head_width = query_pre.shape
    positions = jnp.arange(length, dtype=jnp.float32)
    query_rot = rotate(query_pre, positions).astype(jnp.bfloat16)
    key_rot = rotate(key_pre, positions).astype(jnp.bfloat16)
    value_low = value_pre.astype(jnp.bfloat16)
    blocks = length // BLOCK
    inside = jnp.arange(BLOCK, dtype=jnp.float32)
    distance = inside[:, None] - inside[None, :]
    within = jnp.where(
        distance >= 0, jnp.exp(-decay_rates[:, None, None] * jnp.maximum(distance, 0.0)), 0.0
    ) * head_width ** (-0.5)
    query_blocks = query_rot.reshape(blocks, BLOCK, head_count, head_width)
    key_blocks = key_rot.reshape(blocks, BLOCK, head_count, head_width)
    value_blocks = value_low.reshape(blocks, BLOCK, head_count, head_width)
    scores = jnp.einsum(
        "nihe,njhe->nhij", query_blocks, key_blocks, preferred_element_type=jnp.float32
    )
    weights = (scores * within[None]).astype(jnp.bfloat16)
    inner_part = jnp.einsum(
        "nhij,njhe->nihe", weights, value_blocks, preferred_element_type=jnp.float32
    )
    fading = jnp.exp(-decay_rates[None, :] * (BLOCK - 1.0 - inside[:, None])) * head_width ** (-0.5)
    key_faded = key_blocks.astype(jnp.float32) * fading[None, :, :, None]
    updates = jnp.einsum(
        "njhd,njhe->nhde", key_faded, value_blocks.astype(jnp.float32), precision=HIGHEST
    )
    block_decay = jnp.exp(-decay_rates * BLOCK)

    def advance(memory_state, update):
        return (memory_state * block_decay[:, None, None] + update, memory_state)

    _, before = lax.scan(
        advance, jnp.zeros((head_count, head_width, head_width), jnp.float32), updates
    )
    rising = jnp.exp(-decay_rates[None, :] * (inside[:, None] + 1.0))
    queried = query_blocks.astype(jnp.float32) * rising[None, :, :, None]
    carried_part = jnp.einsum("nihd,nhde->nihe", queried, before, precision=HIGHEST)
    combined = (inner_part + carried_part).reshape(length, head_count, head_width)
    normed = combined * lax.rsqrt(
        jnp.maximum(jnp.mean(combined * combined, axis=-1, keepdims=True), HEAD_FLOOR)
    )
    return normed.astype(jnp.bfloat16).reshape(length, head_count * head_width)


def body(
    residual_in,
    gain_first,
    gain_mixer,
    gain_second,
    gate_weight,
    gate_scale,
    up_weight,
    up_scale,
    down_weight,
    down_scale,
    query_weight,
    query_scale,
    key_weight,
    key_scale,
    value_weight,
    value_scale,
    output_weight,
    output_scale,
):
    gate_part = gate_weight.astype(jnp.bfloat16)
    up_part = up_weight.astype(jnp.bfloat16)
    down_factor, output_factor = (
        lax.all_gather(down_scale, "fs", axis=0, tiled=True),
        lax.all_gather(output_scale, "fs", axis=0, tiled=True),
    )
    first_input = collect_rows(residual_in, gain_first)
    gate_full, up_full = (
        lax.all_gather(gate_part, "fs", axis=0, tiled=True),
        lax.all_gather(up_part, "fs", axis=0, tiled=True),
    )
    gate_pre = jnp.dot(first_input, gate_full, preferred_element_type=jnp.float32)
    up_pre = jnp.dot(first_input, up_full, preferred_element_type=jnp.float32)
    down_full = lax.all_gather(down_weight.astype(jnp.bfloat16), "fs", axis=1, tiled=True)
    hidden_first = (jax.nn.silu(gate_pre * gate_scale) * (up_pre * up_scale)).astype(jnp.bfloat16)
    mlp_first = return_rows(hidden_first, down_full, down_factor)
    middle = (residual_in.astype(jnp.float32) + 0.5 * mlp_first).astype(jnp.bfloat16)
    mixer_input = collect_rows(middle, gain_mixer)
    local_width = query_weight.shape[1]
    projections = (
        query_weight.astype(jnp.bfloat16),
        key_weight.astype(jnp.bfloat16),
        value_weight.astype(jnp.bfloat16),
    )
    pieces = (
        lax.all_gather(projections[0], "fs", axis=0, tiled=True),
        lax.all_gather(projections[1], "fs", axis=0, tiled=True),
        lax.all_gather(projections[2], "fs", axis=0, tiled=True),
    )
    query_pre, key_pre, value_pre = tuple(
        (
            jnp.dot(mixer_input, pieces[member], preferred_element_type=jnp.float32)
            for member in range(3)
        )
    )
    output_full = lax.all_gather(output_weight.astype(jnp.bfloat16), "fs", axis=1, tiled=True)
    length = mixer_input.shape[0]
    heads_local = local_width // HEAD_DIM
    decay_rates = head_rates(lax.axis_index("tp") * heads_local, heads_local, length)
    mixed = retention(
        (query_pre * query_scale).reshape(length, heads_local, HEAD_DIM),
        (key_pre * key_scale).reshape(length, heads_local, HEAD_DIM),
        (value_pre * value_scale).reshape(length, heads_local, HEAD_DIM),
        decay_rates,
    )
    mixer_out = return_rows(mixed, output_full, output_factor)
    second = (middle.astype(jnp.float32) + mixer_out).astype(jnp.bfloat16)
    last_input = collect_rows(second, gain_second)
    gate_last = jnp.dot(last_input, gate_full, preferred_element_type=jnp.float32) * gate_scale
    up_last = jnp.dot(last_input, up_full, preferred_element_type=jnp.float32) * up_scale
    hidden_second = (jax.nn.silu(gate_last) * up_last).astype(jnp.bfloat16)
    mlp_second = return_rows(hidden_second, down_full, down_factor)
    return (second.astype(jnp.float32) + 0.5 * mlp_second).astype(jnp.bfloat16)


def solution(mesh):
    in_specs = (
        P(("fs", "tp"), None),
        P(),
        P(),
        P(),
        P("fs", "tp"),
        P("tp"),
        P("fs", "tp"),
        P("tp"),
        P("tp", "fs"),
        P("fs"),
        P("fs", "tp"),
        P("tp"),
        P("fs", "tp"),
        P("tp"),
        P("fs", "tp"),
        P("tp"),
        P("tp", "fs"),
        P("fs"),
    )
    out_specs = P(("fs", "tp"), None)
    return jax.shard_map(body, mesh=mesh, in_specs=in_specs, out_specs=out_specs, check_vma=False)
```

profile of v0, /device:TPU:0, one launch (start us, length us, event | category | flops | bytes accessed | tf_op | source)
XLA Modules:
  0.0 955.4 jit_solution(6325975038016141110)
XLA Ops:
  7.9 2.0 fusion.14
  10.0 2.4 convert_element_type.119
  13.6 2.4 convert_element_type.122
  16.0 43.0 %all-gather = f32[16,1,128]{2,1,0:T(1,128)S(1)} all-gather(f32[1,1,128]{2,1,0:T(1,128)S(1)} %bitcast.58), channel_id=1, replica_groups=mesh['fs'=16,'tp'=2] {'fs'}, dimensions={0}, use_global_device_ids=true | all-gather | bytes 8704 | tf_op jit(solution)/shard_map/all_gather | solution.py:129
  59.0 118.3 %all-gather.15.cloned.1.call-done = bf16[2048,3072]{1,0:T(8,128)(2,1)} async-done(((bf16[128,3072]{1,0:T(8,128)(2,1)}), bf16[2048,3072]{1,0:T(8,128)(2,1)}) %all-gather.15.cloned.1.call-update) | async-done | bytes 12582928 | tf_op jit(solution)/shard_map/all_gather | solution.py:134
  177.3 9.9 %convolution_multiply_fusion.3 = f32[256,3072]{1,0:T(8,128)} fusion(bf16[256,2048]{1,0:T(8,128)(2,1)} %all-gather.13.cloned.1.call-done, bf16[2048,3072]{1,0:T(8,128)(2,1)} %all-gather.15.cloned.1.call-done, f32[3072]{0:T(1024)S(1)} %copy-done.20), kind=kOutput, calls=%fused_computation.7 | convolution fusion | flops 3222011904 | bytes 16789504 | tf_op jit(solution)/shard_map/dot_general | solution.py:137
  187.2 142.5 %all-gather.17.cloned.1.call-done = bf16[2048,3072]{1,0:T(8,128)(2,1)} async-done(((bf16[128,3072]{1,0:T(8,128)(2,1)}), bf16[2048,3072]{1,0:T(8,128)(2,1)}) %all-gather.17.cloned.1.call-update) | async-done | bytes 12582928 | tf_op jit(solution)/shard_map/all_gather | solution.py:135
  329.7 196.2 %all-gather.19.cloned.1.call-done = bf16[3072,2048]{1,0:T(8,128)(2,1)} async-done(((bf16[3072,128]{1,0:T(8,128)(2,1)}), bf16[3072,2048]{1,0:T(8,128)(2,1)}) %all-gather.19.cloned.1.call-update) | async-done | bytes 12582928 | tf_op jit(solution)/shard_map/all_gather | solution.py:139
  525.9 17.1 %fusion.6 = bf16[256,2048]{1,0:T(8,128)(2,1)} fusion(bf16[3072,2048]{1,0:T(8,128)(2,1)} %all-gather.19.cloned.1.call-done, f32[2048]{0:T(1024)S(1)} %bitcast.56, bf16[256,2048]{1,0:T(8,128)(2,1)S(1)} %copy-done.18, bf16[2048,3072]{1,0:T(8,128)(2,1)} %all-gather.17.cloned.1.call-done, f32[256,3072]{1,0:T(8,128)} %convolution_multiply_fusion.3, ...), kind=kOutput, calls=%fused_computation.15 | convolution fusion | flops 6449004544 | bytes 30429184 | tf_op jit(solution)/shard_map/dot_general | solution.py:28
  544.0 5.9 reduce-scatter.4.cloned.1.call-done
  554.8 41.1 %all-gather.1 = f32[16,1,128]{2,1,0:T(1,128)S(1)} all-gather(f32[1,1,128]{2,1,0:T(1,128)S(1)} %bitcast.59), channel_id=1, replica_groups=mesh['fs'=16,'tp'=2] {'fs'}, dimensions={0}, use_global_device_ids=true | all-gather | bytes 8704 | tf_op jit(solution)/shard_map/all_gather | solution.py:130
  598.0 31.3 %all-gather.25.cloned.1.call-done = bf16[2048,1024]{1,0:T(8,128)(2,1)} async-done(((bf16[128,1024]{1,0:T(8,128)(2,1)}), bf16[2048,1024]{1,0:T(8,128)(2,1)}) %all-gather.25.cloned.1.call-update) | async-done | bytes 4194320 | tf_op jit(solution)/shard_map/all_gather | solution.py:151
  629.2 9.2 all-gather.21.cloned.1.call-done
  638.4 4.7 convolution_multiply_fusion.8
  643.2 1.7 reshape.230
  644.9 73.1 %all-gather.27.cloned.1.call-done = bf16[2048,1024]{1,0:T(8,128)(2,1)} async-done(((bf16[128,1024]{1,0:T(8,128)(2,1)}), bf16[2048,1024]{1,0:T(8,128)(2,1)}) %all-gather.27.cloned.1.call-update) | async-done | bytes 4194320 | tf_op jit(solution)/shard_map/all_gather | solution.py:152
  718.0 4.7 convolution_multiply_fusion.7
  722.7 2.7 reshape.231
  725.4 69.6 %all-gather.23.cloned.1.call-done = bf16[2048,1024]{1,0:T(8,128)(2,1)} async-done(((bf16[128,1024]{1,0:T(8,128)(2,1)}), bf16[2048,1024]{1,0:T(8,128)(2,1)}) %all-gather.23.cloned.1.call-update) | async-done | bytes 4194320 | tf_op jit(solution)/shard_map/all_gather | solution.py:153
  795.0 4.6 fusion.10
  802.8 3.9 fusion.27
  806.7 10.4 %while.13 = (s32[]{:T(128)}, f32[4,256,256]{2,1,0:T(8,128)S(1)}, f32[4,4,256,256]{3,2,1,0:T(8,128)}, f32[4,4,256,256]{3,2,1,0:T(8,128)}, s32[]{:T(128)}, /*index=5*/s32[]{:T(128)}, s32[]{:T(128)}) while((s32[]{:T(128)}, f32[4,256,256]{2,1,0:T(8,128)S(1)}, f32[4,4,256,256]{3,2,1,0:T(8,128)}, f32[4,4,256,256]{3,2,1,0:T(8,128)}, ...), condition=%wide.region_4.5_spmd.clone, body=%wide.region_3.4_spmd.clone.sunk | while | flops 1048603 | bytes 5243520 | solution.py:93
  817.2 5.1 fusion.24
  825.5 59.4 %all-gather.29.cloned.1.call-done = bf16[1024,2048]{1,0:T(8,128)(2,1)} async-done(((bf16[1024,128]{1,0:T(8,128)(2,1)}), bf16[1024,2048]{1,0:T(8,128)(2,1)}) %all-gather.29.cloned.1.call-update) | async-done | bytes 4194320 | tf_op jit(solution)/shard_map/all_gather | solution.py:161
  884.9 4.5 fusion.8
  889.5 6.7 reduce-scatter.6.cloned.1.call-done
  897.5 2.0 fusion.22
  899.9 10.1 %all-gather.31.cloned.1.call-done = bf16[256,2048]{1,0:T(8,128)(2,1)} async-done(((bf16[128,2048]{1,0:T(8,128)(2,1)}), bf16[256,2048]{1,0:T(8,128)(2,1)}) %all-gather.31.cloned.1.call-update) | async-done | bytes 1048592 | tf_op jit(solution)/shard_map/all_gather | solution.py:24
  909.9 10.0 %convolution_multiply_fusion.1 = f32[256,3072]{1,0:T(8,128)} fusion(bf16[256,2048]{1,0:T(8,128)(2,1)} %all-gather.31.cloned.1.call-done, bf16[2048,3072]{1,0:T(8,128)(2,1)} %all-gather.15.cloned.1.call-done, f32[3072]{0:T(1024)S(1)} %copy-done.21), kind=kOutput, calls=%fused_computation.5 | convolution fusion | flops 3222011904 | bytes 16789504 | tf_op jit(solution)/shard_map/dot_general | solution.py:174
  920.0 17.0 %fusion.7 = bf16[256,2048]{1,0:T(8,128)(2,1)} fusion(bf16[3072,2048]{1,0:T(8,128)(2,1)} %all-gather.19.cloned.1.call-done, f32[2048]{0:T(1024)S(1)} %bitcast.57, bf16[256,2048]{1,0:T(8,128)(2,1)S(1)} %copy-done.19, bf16[2048,3072]{1,0:T(8,128)(2,1)} %all-gather.17.cloned.1.call-done, f32[256,3072]{1,0:T(8,128)} %convolution_multiply_fusion.1, ...), kind=kOutput, calls=%fused_computation.16 | convolution fusion | flops 6449004544 | bytes 30429184 | tf_op jit(solution)/shard_map/dot_general | solution.py:28
  937.0 9.7 %reduce-scatter.8.cloned.1.call-done = bf16[128,2048]{1,0:T(8,128)(2,1)} async-done(((bf16[256,2048]{1,0:T(8,128)(2,1)}), bf16[128,2048]{1,0:T(8,128)(2,1)}) %reduce-scatter.8.cloned.1.call-update) | async-done | bytes 524304 | tf_op jit(solution)/shard_map/reduce_scatter | solution.py:29
  946.8 2.1 fusion.23
  (125 shorter events, 28.7 us)
Async XLA Ops:
  6.5 52.5 %all-gather.13.cloned.1.call-start = ((), (), s32[]{:S(2)}) async-start(), calls=%async_computation.3 | async-start | bytes 1572864 | tf_op jit(solution)/shard_map/all_gather | solution.py:24
  10.0 167.3 %copy-start.20 = (f32[3072]{0:T(1024)S(1)}, f32[3072]{0:T(1024)}, u32[]{:S(2)}) copy-start(f32[3072]{0:T(1024)} %param.25) | copy-start | bytes 36868
  10.0 167.3 %all-gather.15.cloned.1.call-start = ((), (), s32[]{:S(2)}) async-start(), calls=%async_computation.4 | async-start | bytes 13369344 | tf_op jit(solution)/shard_map/all_gather | solution.py:134
  12.4 317.3 %all-gather.17.cloned.1.call-start = ((), (), s32[]{:S(2)}) async-start(), calls=%async_computation.5 | async-start | bytes 13369344 | tf_op jit(solution)/shard_map/all_gather | solution.py:135
  13.5 512.4 %all-gather.19.cloned.1.call-start = ((), (), s32[]{:S(2)}) async-start(), calls=%async_computation.6 | async-start | bytes 13369344 | tf_op jit(solution)/shard_map/all_gather | solution.py:139
  16.0 533.8 %reduce-scatter.4.cloned.1.call-start = ((), (), s32[]{:S(2)}) async-start(), calls=%async_computation.7 | async-start | bytes 1572864 | tf_op jit(solution)/shard_map/reduce_scatter | solution.py:29
  59.0 466.9 %copy-start.14 = (f32[16,1,128]{2,1,0:T(1,128)}, f32[16,1,128]{2,1,0:T(1,128)S(1)}, u32[]{:S(2)}) copy-start(f32[16,1,128]{2,1,0:T(1,128)S(1)} %all-gather) | copy-start | bytes 24580
  59.0 466.9 %copy-start.22 = (f32[3072]{0:T(1024)S(1)}, f32[3072]{0:T(1024)}, u32[]{:S(2)}) copy-start(f32[3072]{0:T(1024)} %param.27) | copy-start | bytes 36868
  59.0 466.9 %copy-start.18 = (bf16[256,2048]{1,0:T(8,128)(2,1)S(1)}, bf16[256,2048]{1,0:T(8,128)(2,1)}, u32[]{:S(2)}) copy-start(bf16[256,2048]{1,0:T(8,128)(2,1)} %all-gather.13.cloned.1.call-done) | copy-start | bytes 3145732
  525.9 17.2 %copy-start.6 = (f32[128,1024]{1,0:T(8,128)S(1)}, f32[128,1024]{1,0:T(8,128)}, u32[]{:S(2)}) copy-start(f32[128,1024]{1,0:T(8,128)} %param.30) | copy-start | bytes 1572868
  525.9 23.9 %copy-start = (bf16[128,2048]{1,0:T(8,128)(2,1)S(1)}, bf16[128,2048]{1,0:T(8,128)(2,1)}, u32[]{:S(2)}) copy-start(bf16[128,2048]{1,0:T(8,128)(2,1)} %param.20) | copy-start | bytes 1572868
  525.9 25.2 %copy-start.12 = (f32[2048]{0:T(1024)S(1)}, f32[2048]{0:T(1024)}, u32[]{:S(2)}) copy-start(f32[2048]{0:T(1024)} %param.22) | copy-start | bytes 24580
  543.0 10.9 %copy-start.9 = (f32[1024,128]{1,0:T(8,128)S(1)}, f32[1024,128]{1,0:T(8,128)}, u32[]{:S(2)}) copy-start(f32[1024,128]{1,0:T(8,128)} %param.36) | copy-start | bytes 1572868
  543.0 11.7 %copy-start.17 = (f32[128]{0:T(128)S(1)}, f32[128]{0:T(128)}, u32[]{:S(2)}) copy-start(f32[128]{0:T(128)} %param.37) | copy-start | bytes 1540
  543.1 95.3 %copy-start.24 = (f32[1024]{0:T(1024)S(1)}, f32[1024]{0:T(1024)}, u32[]{:S(2)}) copy-start(f32[1024]{0:T(1024)} %param.31) | copy-start | bytes 12292
  543.1 86.1 %all-gather.25.cloned.1.call-start = ((), (), s32[]{:S(2)}) async-start(), calls=%async_computation.10 | async-start | bytes 4456448 | tf_op jit(solution)/shard_map/all_gather | solution.py:151
  543.9 94.5 %all-gather.21.cloned.1.call-start = ((), (), s32[]{:S(2)}) async-start(), calls=%async_computation.8 | async-start | bytes 1572864 | tf_op jit(solution)/shard_map/all_gather | solution.py:24
  552.2 165.8 %all-gather.27.cloned.1.call-start = ((), (), s32[]{:S(2)}) async-start(), calls=%async_computation.11 | async-start | bytes 4456448 | tf_op jit(solution)/shard_map/all_gather | solution.py:152
  553.0 242.0 %all-gather.23.cloned.1.call-start = ((), (), s32[]{:S(2)}) async-start(), calls=%async_computation.9 | async-start | bytes 4456448 | tf_op jit(solution)/shard_map/all_gather | solution.py:153
  553.9 331.1 %all-gather.29.cloned.1.call-start = ((), (), s32[]{:S(2)}) async-start(), calls=%async_computation.12 | async-start | bytes 4456448 | tf_op jit(solution)/shard_map/all_gather | solution.py:161
  554.7 341.5 %reduce-scatter.6.cloned.1.call-start = ((), (), s32[]{:S(2)}) async-start(), calls=%async_computation.13 | async-start | bytes 1572864 | tf_op jit(solution)/shard_map/reduce_scatter | solution.py:29
  598.0 120.0 %copy-start.25 = (f32[1024]{0:T(1024)S(1)}, f32[1024]{0:T(1024)}, u32[]{:S(2)}) copy-start(f32[1024]{0:T(1024)} %param.33) | copy-start | bytes 12292
  644.9 150.1 %copy-start.26 = (f32[1024]{0:T(1024)S(1)}, f32[1024]{0:T(1024)}, u32[]{:S(2)}) copy-start(f32[1024]{0:T(1024)} %param.35) | copy-start | bytes 12292
  802.8 14.4 %copy-start.4 = (bf16[256,4,128]{2,0,1:T(8,128)(2,1)}, bf16[256,4,128]{2,0,1:T(8,128)(2,1)S(1)}, u32[]{:S(2)}) copy-start(bf16[256,4,128]{2,0,1:T(8,128)(2,1)S(1)} %get-tuple-element.66) | copy-start | bytes 786436
  802.8 14.4 %copy-start.5 = (bf16[256,4,128]{2,0,1:T(8,128)(2,1)}, bf16[256,4,128]{2,0,1:T(8,128)(2,1)S(1)}, u32[]{:S(2)}) copy-start(bf16[256,4,128]{2,0,1:T(8,128)(2,1)S(1)} %get-tuple-element.67) | copy-start | bytes 786436
  884.9 12.5 %copy-start.13 = (f32[2048]{0:T(1024)S(1)}, f32[2048]{0:T(1024)}, u32[]{:S(2)}) copy-start(f32[2048]{0:T(1024)} %param.23) | copy-start | bytes 24580
  884.9 25.0 %copy-start.21 = (f32[3072]{0:T(1024)S(1)}, f32[3072]{0:T(1024)}, u32[]{:S(2)}) copy-start(f32[3072]{0:T(1024)} %param.25) | copy-start | bytes 36868
  889.4 20.5 %all-gather.31.cloned.1.call-start = ((), (), s32[]{:S(2)}) async-start(), calls=%async_computation.14 | async-start | bytes 1572864 | tf_op jit(solution)/shard_map/all_gather | solution.py:24
  899.5 20.4 %copy-start.15 = (f32[16,1,128]{2,1,0:T(1,128)S(1)}, f32[16,1,128]{2,1,0:T(1,128)}, u32[]{:S(2)}) copy-start(f32[16,1,128]{2,1,0:T(1,128)} %copy-done.14) | copy-start | bytes 24580
  899.5 20.4 %copy-start.23 = (f32[3072]{0:T(1024)S(1)}, f32[3072]{0:T(1024)}, u32[]{:S(2)}) copy-start(f32[3072]{0:T(1024)} %param.27) | copy-start | bytes 36868
  899.6 47.2 %reduce-scatter.8.cloned.1.call-start = ((), (), s32[]{:S(2)}) async-start(), calls=%async_computation.15 | async-start | bytes 1572864 | tf_op jit(solution)/shard_map/reduce_scatter | solution.py:29
  920.0 26.8 %copy-start.1 = (bf16[128,2048]{1,0:T(8,128)(2,1)S(1)}, bf16[128,2048]{1,0:T(8,128)(2,1)}, u32[]{:S(2)}) copy-start(bf16[128,2048]{1,0:T(8,128)(2,1)} %reduce-scatter.6.cloned.1.call-done) | copy-start | bytes 1572868
  (8 other events, 51.9 us)
Sparse Core Ops, SparseCore 0:
  10.1 11.7 all-gather.12
  24.6 152.6 all-gather.14
  180.1 149.5 all-gather.16
  332.2 193.6 all-gather.18
  543.2 6.5 reduce-scatter.3
  552.4 76.7 all-gather.24
  630.8 7.6 all-gather.20
  641.2 76.7 all-gather.26
  720.8 74.1 all-gather.22
  797.5 87.3 all-gather.28
  889.6 6.5 reduce-scatter.5
  899.7 10.2 all-gather.30
  937.1 9.5 reduce-scatter.7
where the time goes:
time: 956 us; the launch traced here: 955 us
  waiting for transfers between devices  732 us (77%)
  blocking collectives  84.1 us (9%)
  matrix products  83.2 us (9%)
  other arithmetic  32.5 us (3%)
  between operations  13.6 us (1%)
    all_gather x1, waiting for transfers between devices, body(): lax.all_gather(down_weight.astype(jnp.bfloat16), 'fs', axis=1, tiled=True)  196 us
    all_gather x1, waiting for transfers between devices, body(): lax.all_gather(up_part, 'fs', axis=0, tiled=True)  142 us
    all_gather x1, waiting for transfers between devices, body(): lax.all_gather(gate_part, 'fs', axis=0, tiled=True)  118 us
    all_gather x1, waiting for transfers between devices, body(): lax.all_gather(projections[1], 'fs', axis=0, tiled=True)  73.1 us
    all_gather x1, waiting for transfers between devices, body(): lax.all_gather(projections[2], 'fs', axis=0, tiled=True)  69.6 us
    all_gather x1, waiting for transfers between devices, body(): lax.all_gather(output_weight.astype(jnp.bfloat16), 'fs', axis=1, tiled=True)  59.4 us
    all_gather x1, blocking collectives, body(): lax.all_gather(down_scale, 'fs', axis=0, tiled=True)  43 us
    all_gather x1, blocking collectives, body(): lax.all_gather(output_scale, 'fs', axis=0, tiled=True)  41.1 us
  transfers between devices with their start and end apart: 13, of which 12 were waited for; matrix products, arithmetic and copies ran while one was open for 7% of the time, Pallas kernels for 0%

commit v1 on v0

v1 whole, which is shorter than its diff:
```python
import math

import jax
import jax.numpy as jnp
from jax import lax
from jax.sharding import PartitionSpec as P

HEADS = 8
HEAD_DIM = 256
BLOCK = 64


EPSILON = 1e-06
HEAD_FLOOR = 0.25
ROTARY_BASE = 10000.0
HIGHEST = lax.Precision.HIGHEST


def normalize(sequence_rows, gain_vector):
    values = sequence_rows.astype(jnp.float32)
    scaled = values * lax.rsqrt(jnp.mean(values * values, axis=-1, keepdims=True) + EPSILON)
    return (scaled * gain_vector).astype(jnp.bfloat16)


def head_rates(first_head, head_count, length):
    head_number = (first_head + jnp.arange(head_count)).astype(jnp.float32)
    return jnp.exp(jnp.log(1.0 / 16.0) + head_number / (HEADS - 1) * jnp.log(4.0 / length))


def rotate(values, positions):
    half_width = values.shape[-1] // 2
    frequency = ROTARY_BASE ** (-jnp.arange(half_width, dtype=jnp.float32) * 2.0 / values.shape[-1])
    angles = positions[:, None] * frequency[None, :]
    cosine = jnp.cos(angles)[:, None, :]
    sine_value = jnp.sin(angles)[:, None, :]
    front_half = values[..., :half_width]
    back_half = values[..., half_width:]
    return jnp.concatenate(
        [
            front_half * cosine - back_half * sine_value,
            back_half * cosine + front_half * sine_value,
        ],
        axis=-1,
    )


def retention(query_pre, key_pre, value_pre, decay_rates):
    length, head_count, head_width = query_pre.shape
    positions = jnp.arange(length, dtype=jnp.float32)
    query_rot = rotate(query_pre, positions).astype(jnp.bfloat16)
    key_rot = rotate(key_pre, positions).astype(jnp.bfloat16)
    value_low = value_pre.astype(jnp.bfloat16)
    blocks = length // BLOCK
    inside = jnp.arange(BLOCK, dtype=jnp.float32)
    distance = inside[:, None] - inside[None, :]
    within = jnp.where(
        distance >= 0, jnp.exp(-decay_rates[:, None, None] * jnp.maximum(distance, 0.0)), 0.0
    ) * head_width ** (-0.5)
    query_blocks = query_rot.reshape(blocks, BLOCK, head_count, head_width)
    key_blocks = key_rot.reshape(blocks, BLOCK, head_count, head_width)
    value_blocks = value_low.reshape(blocks, BLOCK, head_count, head_width)
    scores = jnp.einsum(
        "nihe,njhe->nhij", query_blocks, key_blocks, preferred_element_type=jnp.float32
    )
    weights = (scores * within[None]).astype(jnp.bfloat16)
    inner_part = jnp.einsum(
        "nhij,njhe->nihe", weights, value_blocks, preferred_element_type=jnp.float32
    )
    fading = jnp.exp(-decay_rates[None, :] * (BLOCK - 1.0 - inside[:, None])) * head_width ** (-0.5)
    key_faded = key_blocks.astype(jnp.float32) * fading[None, :, :, None]
    updates = jnp.einsum(
        "njhd,njhe->nhde", key_faded, value_blocks.astype(jnp.float32), precision=HIGHEST
    )
    block_decay = jnp.exp(-decay_rates * BLOCK)

    def advance(memory_state, update):
        return (memory_state * block_decay[:, None, None] + update, memory_state)

    _, before = lax.scan(
        advance, jnp.zeros((head_count, head_width, head_width), jnp.float32), updates
    )
    rising = jnp.exp(-decay_rates[None, :] * (inside[:, None] + 1.0))
    queried = query_blocks.astype(jnp.float32) * rising[None, :, :, None]
    carried_part = jnp.einsum("nihd,nhde->nihe", queried, before, precision=HIGHEST)
    combined = (inner_part + carried_part).reshape(length, head_count, head_width)
    normed = combined * lax.rsqrt(
        jnp.maximum(jnp.mean(combined * combined, axis=-1, keepdims=True), HEAD_FLOOR)
    )
    return normed.astype(jnp.bfloat16).reshape(length, head_count * head_width)


def split_three(values):
    high = values.astype(jnp.bfloat16)
    rest = values - high.astype(jnp.float32)
    middle_part = rest.astype(jnp.bfloat16)
    low = (rest - middle_part.astype(jnp.float32)).astype(jnp.bfloat16)
    return [high, middle_part, low]


def make_body(n_fs, n_tp, share):
    spread = n_fs // share
    STRIDED = False
    if STRIDED:
        teams = [[m * spread + r for m in range(share)] for r in range(spread)]
    else:
        teams = [[r * share + m for m in range(share)] for r in range(spread)]
    twins = [[team[m] for team in teams] for m in range(share)]
    row_teams = [[f * n_tp + t for f in team for t in range(n_tp)] for team in teams]

    def my_rank():
        position = lax.axis_index("fs")
        return position // spread if STRIDED else position % share

    def fetch(pieces):
        swapped = lax.all_to_all(
            pieces, "fs", split_axis=0, concat_axis=0, axis_index_groups=teams, tiled=True
        )
        return lax.all_gather(swapped, "fs", axis=0, axis_index_groups=twins, tiled=False)

    def order_features(rows):
        if not STRIDED:
            return rows
        count = rows.shape[0]
        return rows.reshape(count, share, spread, -1).swapaxes(1, 2).reshape(count, -1)

    def collect_rows(rows, gain_vector):
        return lax.all_gather(
            order_features(normalize(rows, gain_vector)),
            ("fs", "tp"),
            axis=0,
            axis_index_groups=row_teams,
            tiled=True,
        )

    def return_rows(inputs, weight, factor):
        term = jnp.dot(inputs, weight, preferred_element_type=jnp.float32) * factor
        return lax.psum_scatter(
            term.astype(jnp.bfloat16),
            ("fs", "tp"),
            scatter_dimension=0,
            axis_index_groups=row_teams,
            tiled=True,
        ).astype(jnp.float32)

    def columns_of(weight):
        low = weight.astype(jnp.bfloat16)
        return low.reshape(low.shape[0], share, -1).swapaxes(0, 1)

    def rows_of(weight):
        low = weight.astype(jnp.bfloat16)
        return low.reshape(share, -1, low.shape[1])

    def own(vector, rank):
        width = vector.shape[0] // share
        return lax.dynamic_slice_in_dim(vector, rank * width, width)

    def body(
        residual_in,
        gain_first,
        gain_mixer,
        gain_second,
        gate_weight,
        gate_scale,
        up_weight,
        up_scale,
        down_weight,
        down_scale,
        query_weight,
        query_scale,
        key_weight,
        key_scale,
        value_weight,
        value_scale,
        output_weight,
        output_scale,
    ):
        rank = my_rank()
        hidden_width = gate_weight.shape[1] // share
        mix_width = query_weight.shape[1] // share
        entry = fetch(jnp.concatenate([columns_of(gate_weight), columns_of(up_weight)], axis=2))
        factors = split_three(down_scale) + split_three(output_scale)
        factors = jnp.stack(factors + [jnp.zeros_like(factors[0])] * 10)
        leave_piece = jnp.concatenate(
            [
                rows_of(down_weight),
                rows_of(output_weight),
                jnp.broadcast_to(factors[None], (share,) + factors.shape),
            ],
            axis=1,
        )
        first_input = collect_rows(residual_in, gain_first)
        leave_piece, entry = lax.optimization_barrier((leave_piece, entry)) if False else (leave_piece, entry)
        leave = fetch(leave_piece)
        project_piece = jnp.concatenate(
            [columns_of(query_weight), columns_of(key_weight), columns_of(value_weight)], axis=2
        )
        project_piece, leave = lax.optimization_barrier((project_piece, leave)) if False else (project_piece, leave)
        project = fetch(project_piece)

        entry = entry.reshape(-1, 2 * hidden_width)
        project = project.reshape(-1, 3 * mix_width)
        if STRIDED:
            leave = leave.swapaxes(0, 1)
        leave = leave.transpose(2, 0, 1, 3).reshape(leave.shape[2], -1)
        down_full = leave[:hidden_width]
        output_full = leave[hidden_width : hidden_width + mix_width]
        parts = leave[hidden_width + mix_width :].astype(jnp.float32)
        down_factor = parts[0] + parts[1] + parts[2]
        output_factor = parts[3] + parts[4] + parts[5]
        gate_own, up_own = own(gate_scale, rank), own(up_scale, rank)

        def half_step(inputs):
            both = jnp.dot(inputs, entry, preferred_element_type=jnp.float32)
            gate_pre = both[:, :hidden_width] * gate_own
            up_pre = both[:, hidden_width:] * up_own
            hidden = (jax.nn.silu(gate_pre) * up_pre).astype(jnp.bfloat16)
            return return_rows(hidden, down_full, down_factor)

        mlp_first = half_step(first_input)
        middle = (residual_in.astype(jnp.float32) + 0.5 * mlp_first).astype(jnp.bfloat16)
        mixer_input = collect_rows(middle, gain_mixer)
        both = jnp.dot(mixer_input, project, preferred_element_type=jnp.float32)
        scale = jnp.concatenate([own(v, rank) for v in (query_scale, key_scale, value_scale)])
        length = residual_in.shape[0] * n_tp
        heads_own = mix_width // HEAD_DIM
        both = (both * scale).reshape(share, length, 3, heads_own, HEAD_DIM)
        first_head = (lax.axis_index("tp") * share + rank) * heads_own
        decay_rates = head_rates(first_head, heads_own, length)
        mixed = jax.vmap(lambda t: retention(t[:, 0], t[:, 1], t[:, 2], decay_rates))(both)
        mixer_out = return_rows(mixed.reshape(share * length, mix_width), output_full, output_factor)
        second = (middle.astype(jnp.float32) + mixer_out).astype(jnp.bfloat16)
        mlp_second = half_step(collect_rows(second, gain_second))
        return (second.astype(jnp.float32) + 0.5 * mlp_second).astype(jnp.bfloat16)

    return body


def solution(mesh):
    n_fs, n_tp = mesh.shape["fs"], mesh.shape["tp"]
    share = math.gcd(math.gcd(HEADS // n_tp, n_fs), 4)
    body = make_body(n_fs, n_tp, share)
    in_specs = (
        P(("fs", "tp"), None),
        P(),
        P(),
        P(),
        P("fs", "tp"),
        P("tp"),
        P("fs", "tp"),
        P("tp"),
        P("tp", "fs"),
        P("fs"),
        P("fs", "tp"),
        P("tp"),
        P("fs", "tp"),
        P("tp"),
        P("fs", "tp"),
        P("tp"),
        P("tp", "fs"),
        P("fs"),
    )
    out_specs = P(("fs", "tp"), None)
    return jax.shard_map(body, mesh=mesh, in_specs=in_specs, out_specs=out_specs, check_vma=False)
```

time: 956 us -> 653 us (0.68)
  waiting for transfers between devices: 732 us -> 455 us
  local copies, waits for them, and re-layouts: 8.91 us -> 43.4 us
  matrix products: 83.2 us -> 52.5 us
  blocking collectives: 84.1 us -> 56 us
    all_gather x10 -> x6, waiting for transfers between devices: 710 us -> 321 us  [the longest x3 224 us: fetch(): lax.all_gather(swapped, 'fs', axis=0, axis_index_groups=twins, tiled=False)]
    reduce_scatter x3, waiting for transfers between devices: 22.3 us -> 134 us  [return_rows(): lax.psum_scatter(term.astype(jnp.bfloat16), ('fs', 'tp'), scatter_dimensi...]
    all_gather x2 -> x0, blocking collectives: 84.1 us -> none  [the longest x1 43 us: body(): lax.all_gather(down_scale, 'fs', axis=0, tiled=True)]
    all_to_all x0 -> x3, blocking collectives: none -> 56 us  [fetch(): lax.all_to_all(pieces, 'fs', split_axis=0, concat_axis=0, axis_index_grou...]
    dot_general x3, matrix products: 38.6 us -> 13.6 us  [return_rows(): term = jnp.dot(inputs, weight, preferred_element_type=jnp.float32) * factor]
    dot_general x5 -> x3, matrix products: 34 us -> 28.6 us  [the longest x2 20.3 us: half_step(): both = jnp.dot(inputs, entry, preferred_element_type=jnp.float32)]
  transfers between devices with their start and end apart: 13 -> 9, of which waited for: 12 -> 9; matrix products, arithmetic and copies ran while one was open for 7% -> 5% of each run, Pallas kernels for 0% -> 0%
where the time goes in v1:
time: 653 us; the launch traced here: 652 us
  waiting for transfers between devices  455 us (70%)
  blocking collectives  56 us (9%)
  matrix products  52.5 us (8%)
  local copies, waits for them, and re-layouts  43.4 us (7%)
  other arithmetic  30.5 us (5%)
  between operations  13.7 us (2%)
    all_gather x3, waiting for transfers between devices, fetch(): lax.all_gather(swapped, 'fs', axis=0, axis_index_groups=twins, tiled=False)  224 us
    reduce_scatter x3, waiting for transfers between devices, return_rows(): lax.psum_scatter(term.astype(jnp.bfloat16), ('fs', 'tp'), scatter_dimensi...  134 us
    all_gather x3, waiting for transfers between devices, collect_rows(): lax.all_gather(order_features(normalize(rows, gain_vector)), ('fs', 'tp')...  96.9 us
    all_to_all x3, blocking collectives, fetch(): lax.all_to_all(pieces, 'fs', split_axis=0, concat_axis=0, axis_index_grou...  56 us
    dot_general x2, matrix products, half_step(): both = jnp.dot(inputs, entry, preferred_element_type=jnp.float32)  20.3 us
    dot_general x3, matrix products, return_rows(): term = jnp.dot(inputs, weight, preferred_element_type=jnp.float32) * factor  13.6 us
  transfers between devices with their start and end apart: 9, of which 9 were waited for; matrix products, arithmetic and copies ran while one was open for 5% of the time, Pallas kernels for 0%

profile of v1, /device:TPU:0, one launch (start us, length us, event | category | flops | bytes accessed | tf_op | source)
XLA Modules:
  0.0 651.8 jit_solution(6444827815063190604)
XLA Ops:
  9.3 19.7 %all_to_all.15 = bf16[4,1040,128]{2,1,0:T(8,128)(2,1)} all-to-all(bf16[4,1040,128]{2,1,0:T(8,128)(2,1)S(1)} %pad_maximum_fusion.1), channel_id=1, replica_groups={{0,2,4,6},{8,10,12,14},{16,18,20,22},{24,26,28,30},{1,3,5,7},{9,11,13,1..., dimensions={0} | all-to-all | bytes 2129920 | tf_op jit(solution)/shard_map/all_to_all | solution.py:115
  30.4 1.8 copy.71
  34.1 21.3 %all_to_all.16 = bf16[4,128,1536]{1,2,0:T(8,128)(2,1)S(1)} all-to-all(bf16[4,128,1536]{1,2,0:T(8,128)(2,1)S(1)} %pad_maximum_fusion), channel_id=1, replica_groups={{0,2,4,6},{8,10,12,14},{16,18,20,22},{24,26,28,30},{1,3,5,7},{9,11,13,1..., dimensions={0} | all-to-all | bytes 3145728 | tf_op jit(solution)/shard_map/all_to_all | solution.py:115
  58.6 51.9 %all-gather.18.cloned.1.call-done = bf16[16,1040,128]{2,1,0:T(8,128)(2,1)} async-done(((bf16[4,1040,128]{2,1,0:T(8,128)(2,1)}), bf16[16,1040,128]{2,1,0:T(8,128)(2,1)}) %all-gather.18.cloned.1.call-update) | async-done | bytes 4259856 | tf_op jit(solution)/shard_map/all_gather | solution.py:118
  110.5 6.4 copy.74
  116.9 4.1 slice.98
  122.1 2.0 fusion.35
  124.2 23.3 %all-gather.10.cloned.1.call-done = bf16[1024,2048]{1,0:T(8,128)(2,1)} async-done(((bf16[128,2048]{1,0:T(8,128)(2,1)}), bf16[1024,2048]{1,0:T(8,128)(2,1)}) %all-gather.10.cloned.1.call-update) | async-done | bytes 4194320 | tf_op jit(solution)/shard_map/all_gather | solution.py:127
  147.5 116.9 %all-gather.16.cloned.1.call-done = bf16[16,128,1536]{2,1,0:T(8,128)(2,1)} async-done(((bf16[4,128,1536]{2,1,0:T(8,128)(2,1)}), bf16[16,128,1536]{2,1,0:T(8,128)(2,1)}) %all-gather.16.cloned.1.call-update) | async-done | bytes 6291472 | tf_op jit(solution)/shard_map/all_gather | solution.py:118
  264.4 10.1 %fusion.54 = f32[1024,1536]{1,0:T(8,128)S(1)} fusion(bf16[1024,2048]{1,0:T(8,128)(2,1)} %all-gather.10.cloned.1.call-done, bf16[2048,1536]{1,0:T(8,128)(2,1)} %bitcast.133), kind=kOutput, calls=%fused_computation.106 | convolution fusion | flops 6442450944 | bytes 16777216 | tf_op jit(solution)/shard_map/dot_general | solution.py:213
  274.6 5.1 multiply_convert_fusion.2
  281.3 15.0 %all_to_all.17 = bf16[4,128,768]{1,2,0:T(8,128)(2,1)S(1)} all-to-all(bf16[4,128,768]{1,2,0:T(8,128)(2,1)S(1)} %pad_maximum_fusion.2), channel_id=1, replica_groups={{0,2,4,6},{8,10,12,14},{16,18,20,22},{24,26,28,30},{1,3,5,7},{9,11,13,1..., dimensions={0} | all-to-all | bytes 1572864 | tf_op jit(solution)/shard_map/all_to_all | solution.py:115
  297.5 31.7 %reduce-scatter.4.cloned.1.call-done = bf16[128,2048]{1,0:T(8,128)(2,1)} async-done(((bf16[1024,2048]{1,0:T(8,128)(2,1)}), bf16[128,2048]{1,0:T(8,128)(2,1)}) %reduce-scatter.4.cloned.1.call-update) | async-done | bytes 524304 | tf_op jit(solution)/shard_map/reduce_scatter | solution.py:137
  336.6 2.4 slice.110
  339.0 55.1 %all-gather.20.cloned.1.call-done = bf16[16,128,768]{2,1,0:T(8,128)(2,1)} async-done(((bf16[4,128,768]{2,1,0:T(8,128)(2,1)}), bf16[16,128,768]{2,1,0:T(8,128)(2,1)}) %all-gather.20.cloned.1.call-update) | async-done | bytes 3145744 | tf_op jit(solution)/shard_map/all_gather | solution.py:118
  394.1 37.0 %all-gather.12.cloned.1.call-done = bf16[1024,2048]{1,0:T(8,128)(2,1)} async-done(((bf16[128,2048]{1,0:T(8,128)(2,1)}), bf16[1024,2048]{1,0:T(8,128)(2,1)}) %all-gather.12.cloned.1.call-update) | async-done | bytes 4194320 | tf_op jit(solution)/shard_map/all_gather | solution.py:127
  431.1 8.3 %convolution_multiply_fusion = f32[1024,768]{1,0:T(8,128)} fusion(bf16[1024,2048]{1,0:T(8,128)(2,1)} %all-gather.12.cloned.1.call-done, bf16[2048,768]{1,0:T(8,128)(2,1)} %bitcast.135, f32[768]{0:T(1024)S(1)} %pad_maximum_fusion.11), kind=kOutput, calls=%fused_computation.18 | convolution fusion | flops 3222011904 | bytes 10488832 | tf_op jit(solution)/shard_map/dot_general | solution.py:222
  439.4 3.5 copy.79
  442.9 5.2 reshape.332
  448.2 2.2 slice.162
  454.5 2.4 subtract_convert_fusion.1
  460.6 4.7 convolution_bitcast_fusion
  465.3 10.6 %while.13 = (s32[]{:T(128)}, f32[4,1,256,256]{3,2,1,0:T(8,128)S(1)}, f32[4,4,1,256,256]{4,3,1,2,0:T(8,128)}, f32[1]{0:T(128)}, f32[4,4,1,256,256]{4,3,0,1,2:T(8,128)}, /*index=5*/s32[]{:T(128)}, s32[]{:T(128)}) while((s32[]{:T(128)}, f32[4,1,256,256]{3,2,1,0:T(8,128)S(1)}, f32[4,4,1,256,256]{4,3,1,2,0:T(8,128)}, f32[1]{0:T(128)}, ...), condition=%wide.region_4.5_spmd.clone, body=%wide.region_3.4_spmd.clone.sunk | while | flops 1048579 | bytes 5242988 | solution.py:79
  476.3 5.2 multiply_reduce_fusion
  481.8 3.4 multiply_convert_fusion.1
  485.2 51.2 %reduce-scatter.6.cloned.1.call-done = bf16[128,2048]{1,0:T(8,128)(2,1)} async-done(((bf16[1024,2048]{1,0:T(8,128)(2,1)}), bf16[128,2048]{1,0:T(8,128)(2,1)}) %reduce-scatter.6.cloned.1.call-update) | async-done | bytes 524304 | tf_op jit(solution)/shard_map/reduce_scatter | solution.py:137
  537.8 2.0 fusion.33
  539.9 36.7 %all-gather.14.cloned.1.call-done = bf16[1024,2048]{1,0:T(8,128)(2,1)} async-done(((bf16[128,2048]{1,0:T(8,128)(2,1)}), bf16[1024,2048]{1,0:T(8,128)(2,1)}) %all-gather.14.cloned.1.call-update) | async-done | bytes 4194320 | tf_op jit(solution)/shard_map/all_gather | solution.py:127
  576.6 10.1 %fusion.55 = f32[1024,1536]{1,0:T(8,128)S(1)} fusion(bf16[1024,2048]{1,0:T(8,128)(2,1)} %all-gather.14.cloned.1.call-done, bf16[2048,1536]{1,0:T(8,128)(2,1)} %bitcast.134), kind=kOutput, calls=%fused_computation.107 | convolution fusion | flops 6442450944 | bytes 16777216 | tf_op jit(solution)/shard_map/dot_general | solution.py:213
  586.8 5.1 multiply_convert_fusion
  591.9 51.3 %reduce-scatter.8.cloned.1.call-done = bf16[128,2048]{1,0:T(8,128)(2,1)} async-done(((bf16[1024,2048]{1,0:T(8,128)(2,1)}), bf16[128,2048]{1,0:T(8,128)(2,1)}) %reduce-scatter.8.cloned.1.call-update) | async-done | bytes 524304 | tf_op jit(solution)/shard_map/reduce_scatter | solution.py:137
  643.2 2.1 fusion.34
  (111 shorter events, 40.8 us)
Async XLA Ops:
  6.5 2.6 copy-start.17
  6.5 2.6 copy-start.18
  6.5 103.9 %all-gather.18.cloned.1.call-start = ((), (), s32[]{:S(2)}) async-start(), calls=%async_computation.13 | async-start | bytes 5324800 | tf_op jit(solution)/shard_map/all_gather | solution.py:118
  9.1 20.0 %copy-start = (bf16[128,2048]{1,0:T(8,128)(2,1)S(1)}, bf16[128,2048]{1,0:T(8,128)(2,1)}, u32[]{:S(2)}) copy-start(bf16[128,2048]{1,0:T(8,128)(2,1)} %param.20) | copy-start | bytes 1572868
  9.2 20.2 %copy-start.9 = (f32[2048]{0:T(1024)S(1)}, f32[2048]{0:T(1024)}, u32[]{:S(2)}) copy-start(f32[2048]{0:T(1024)} %param.21) | copy-start | bytes 24580
  29.1 118.4 %all-gather.10.cloned.1.call-start = ((), (), s32[]{:S(2)}) async-start(), calls=%async_computation.6 | async-start | bytes 4718592 | tf_op jit(solution)/shard_map/all_gather | solution.py:127
  30.4 234.0 %all-gather.16.cloned.1.call-start = ((), (), s32[]{:S(2)}) async-start(), calls=%async_computation.12 | async-start | bytes 7864320 | tf_op jit(solution)/shard_map/all_gather | solution.py:118
  57.0 272.2 %reduce-scatter.4.cloned.1.call-start = ((), (), s32[]{:S(2)}) async-start(), calls=%async_computation.7 | async-start | bytes 4718592 | tf_op jit(solution)/shard_map/reduce_scatter | solution.py:137
  57.8 216.7 %copy-start.12 = (f32[768]{0:T(1024)}, f32[768]{0:T(1024)S(1)}, u32[]{:S(2)}) copy-start(f32[768]{0:T(1024)S(1)} %dynamic_slice.19) | copy-start | bytes 9220
  58.6 215.9 %copy-start.14 = (f32[768]{0:T(1024)}, f32[768]{0:T(1024)S(1)}, u32[]{:S(2)}) copy-start(f32[768]{0:T(1024)S(1)} %dynamic_slice.20) | copy-start | bytes 9220
  264.4 10.2 %copy-start.2 = (bf16[768,4,4,128]{0,3,2,1:T(8,128)(2,1)S(1)}, bf16[768,4,4,128]{0,3,2,1:T(8,128)(2,1)}, u32[]{:S(2)}) copy-start(bf16[768,4,4,128]{0,3,2,1:T(8,128)(2,1)} %slice.98) | copy-start | bytes 9437188
  279.7 1.0 copy-start.5
  279.7 1.2 copy-start.6
  279.7 1.4 copy-start.7
  279.7 114.4 %all-gather.20.cloned.1.call-start = ((), (), s32[]{:S(2)}) async-start(), calls=%async_computation.14 | async-start | bytes 3932160 | tf_op jit(solution)/shard_map/all_gather | solution.py:118
  281.3 49.3 %copy-start.10 = (f32[2048]{0:T(1024)S(1)}, f32[2048]{0:T(1024)}, u32[]{:S(2)}) copy-start(f32[2048]{0:T(1024)} %param.22) | copy-start | bytes 24580
  297.5 133.6 %all-gather.12.cloned.1.call-start = ((), (), s32[]{:S(2)}) async-start(), calls=%async_computation.8 | async-start | bytes 4718592 | tf_op jit(solution)/shard_map/all_gather | solution.py:127
  331.6 204.9 %reduce-scatter.6.cloned.1.call-start = ((), (), s32[]{:S(2)}) async-start(), calls=%async_computation.9 | async-start | bytes 4718592 | tf_op jit(solution)/shard_map/reduce_scatter | solution.py:137
  465.2 10.6 %copy-start.8 = (f32[64,64]{1,0:T(8,128)S(1)}, f32[64,64]{1,0:T(8,128)}, u32[]{:S(2)}) copy-start(f32[64,64]{1,0:T(8,128)} %select_multiply_fusion) | copy-start | bytes 49156
  465.3 11.1 %copy-start.16 = (f32[64]{0:T(128)S(1)}, f32[64]{0:T(128)}, u32[]{:S(2)}) copy-start(f32[64]{0:T(128)} %get-tuple-element.124) | copy-start | bytes 772
  476.3 5.5 copy-start.4
  485.2 52.6 %copy-start.11 = (f32[2048]{0:T(1024)S(1)}, f32[2048]{0:T(1024)}, u32[]{:S(2)}) copy-start(f32[2048]{0:T(1024)} %param.23) | copy-start | bytes 24580
  485.2 91.4 %all-gather.14.cloned.1.call-start = ((), (), s32[]{:S(2)}) async-start(), calls=%async_computation.10 | async-start | bytes 4718592 | tf_op jit(solution)/shard_map/all_gather | solution.py:127
  539.9 46.9 %copy-start.13 = (f32[768]{0:T(1024)S(1)}, f32[768]{0:T(1024)}, u32[]{:S(2)}) copy-start(f32[768]{0:T(1024)} %copy-done.12) | copy-start | bytes 9220
  539.9 46.9 %copy-start.15 = (f32[768]{0:T(1024)S(1)}, f32[768]{0:T(1024)}, u32[]{:S(2)}) copy-start(f32[768]{0:T(1024)} %copy-done.14) | copy-start | bytes 9220
  539.9 103.3 %reduce-scatter.8.cloned.1.call-start = ((), (), s32[]{:S(2)}) async-start(), calls=%async_computation.11 | async-start | bytes 4718592 | tf_op jit(solution)/shard_map/reduce_scatter | solution.py:137
  576.6 10.2 %copy-start.3 = (bf16[768,4,4,128]{0,3,2,1:T(8,128)(2,1)S(1)}, bf16[768,4,4,128]{0,3,2,1:T(8,128)(2,1)}, u32[]{:S(2)}) copy-start(bf16[768,4,4,128]{0,3,2,1:T(8,128)(2,1)} %slice.98) | copy-start | bytes 9437188
  591.9 51.3 %copy-start.1 = (bf16[128,2048]{1,0:T(8,128)(2,1)S(1)}, bf16[128,2048]{1,0:T(8,128)(2,1)}, u32[]{:S(2)}) copy-start(bf16[128,2048]{1,0:T(8,128)(2,1)} %reduce-scatter.6.cloned.1.call-done) | copy-start | bytes 1572868
Sparse Core Ops, SparseCore 0:
  29.2 81.2 all-gather.17
  112.4 35.0 all-gather.9
  149.0 115.3 all-gather.15
  279.8 49.3 reduce-scatter.3
  330.6 63.4 all-gather.19
  395.8 35.2 all-gather.11
  485.3 51.1 reduce-scatter.5
  540.0 36.5 all-gather.13
  592.0 51.1 reduce-scatter.7
